TPU v7x, 32 devices: a whole 2x2x4 slice. The times are simulated.
32 devices in a mesh: sp: 8 (over z, x), tp: 4 (over y, core).
Axes of the slice: x: 2, y: 2, z: 4, core: 2. Of those that a mesh axis runs over, the one named last changes fastest.
Arguments:
- tokens: bfloat16 [1024, 2048], P('sp', 'tp'), may hold values from -6 to 6
- conv_value_weight: bfloat16 [2048, 1024], P('sp', 'tp'), may hold values from -0.125 to 0.125
- conv_gate_weight: bfloat16 [2048, 1024], P('sp', 'tp'), may hold values from -0.125 to 0.125
- conv_kernel: bfloat16 [31, 1024], P(None, 'tp'), may hold values from -16 to 16
- conv_norm_gain: float32 [1024], P('tp'), may hold values from 0.1 to 1.9
- query_weight: bfloat16 [2048, 2048], P('sp', 'tp'), may hold values from -0.125 to 0.125
- key_weight: bfloat16 [2048, 2048], P('sp', 'tp'), may hold values from -0.125 to 0.125
- value_weight: bfloat16 [2048, 2048], P('sp', 'tp'), may hold values from -0.125 to 0.125
- input_gate_weight: bfloat16 [2048, 8], P(None, 'tp'), may hold values from -0.125 to 0.125
- forget_gate_weight: bfloat16 [2048, 8], P(None, 'tp'), may hold values from -0.125 to 0.125
- input_offset: float32 [1024, 8], P('sp', 'tp'), may hold values from -4 to 210
- forget_offset: float32 [1024, 8], P('sp', 'tp'), may hold values from 0 to 30
- memory_norm_gain: float32 [2048], P('tp'), may hold values from 0.1 to 1.9
- conv_out_weight: bfloat16 [1024, 2048], P('tp', 'sp'), may hold values from -0.3125 to 0.3125
- memory_out_weight: bfloat16 [2048, 2048], P('tp', 'sp'), may hold values from -0.125 to 0.125
Outputs:
- mixed: bfloat16 [1024, 2048], P('sp', 'tp')
All inputs are finite; a program needn't handle non-finite values.
Results may differ from a plain program's by a relative error of at most 0.03.
Values may be sent and summed in bfloat16 or wider, within the bound.
A program may use at most 128 MiB of HBM per device.

v0:
```python
import jax
import jax.numpy as jnp
from jax import lax
from jax.sharding import PartitionSpec as P

BLOCK = 64
EPS = 1e-06
LOWEST_LEVEL = -1e30


def shifted_2(value, axis, steps):
    count = lax.axis_size(axis)
    leading, last = (max(0, -steps), min(count, count - steps))
    return lax.ppermute(value, axis, [(source, source + steps) for source in range(leading, last)])


def carried_in(shard, axis, join, neutral):
    place = lax.axis_index(axis)
    gathered = jax.tree.map(
        lambda a, kind: lax.all_gather(a.astype(kind), axis),
        shard,
        (jnp.bfloat16, jnp.bfloat16, jnp.bfloat16, jnp.bfloat16),
    )
    state = jax.tree.map(lambda a, e: jnp.zeros_like(a) + jnp.asarray(e, a.dtype), shard, neutral)

    def one(step, state):
        return join(
            state,
            jax.tree.map(
                lambda a, own: lax.dynamic_index_in_dim(a, step, 0, False).astype(own.dtype),
                gathered,
                shard,
            ),
        )

    return lax.fori_loop(0, place, one, state)


def block_step(carry, inputs):
    state, normal, level = carry
    query, key, value, gate_in, forget_log = inputs
    length = gate_in.shape[-1]
    scale = query.shape[-1] ** (-0.5)
    causal = jnp.tril(jnp.ones((length, length), dtype=bool))
    within = jnp.cumsum(forget_log, axis=-1)
    log_weight = within[:, :, None] - within[:, None, :] + gate_in[:, None, :]
    log_weight = jnp.where(causal, log_weight, -jnp.inf)
    carried = within + level[:, None]
    top = jnp.maximum(carried, jnp.max(log_weight, axis=-1))
    weight = jnp.exp(log_weight - top[:, :, None])
    carried_weight = jnp.exp(carried - top) * scale
    scores = jnp.einsum("htd,hsd->hts", query, key, preferred_element_type=jnp.float32) * (
        scale * weight
    )
    numer = jnp.einsum(
        "hts,hse->hte", scores.astype(jnp.bfloat16), value, preferred_element_type=jnp.float32
    )
    numer = numer + carried_weight[:, :, None] * jnp.einsum(
        "hed,htd->hte", state.astype(jnp.bfloat16), query, preferred_element_type=jnp.float32
    )
    denom = jnp.sum(scores, axis=-1) + carried_weight * jnp.einsum(
        "hd,htd->ht", normal.astype(jnp.bfloat16), query, preferred_element_type=jnp.float32
    )
    result = numer / jnp.maximum(jnp.abs(denom), 1.0)[:, :, None]
    last = within[:, -1]
    end_log = last[:, None] - within + gate_in
    new_level = jnp.maximum(last + level, jnp.max(end_log, axis=-1))
    keep = jnp.exp(last + level - new_level)
    fresh = jnp.exp(end_log - new_level[:, None])
    scaled_key = (fresh[:, :, None] * key).astype(jnp.bfloat16)
    new_state = keep[:, None, None] * state + jnp.einsum(
        "hse,hsd->hed", value, scaled_key, preferred_element_type=jnp.float32
    )
    new_normal = keep[:, None] * normal + jnp.sum(scaled_key.astype(jnp.float32), axis=1)
    return ((new_state, new_normal, new_level), result)


def depthwise(extended, kernel):
    taps = kernel.shape[0]
    length = extended.shape[0] - taps + 1
    total = extended[0:length] * kernel[0]
    for index in range(1, taps):
        total = total + extended[index : index + length] * kernel[index]
    return total


def merge_states(first, second):
    first_state, first_normal, first_level, first_total = first
    second_state, second_normal, second_level, second_total = second
    shifted = first_level + second_total
    level = jnp.maximum(shifted, second_level)
    older = jnp.exp(shifted - level)
    newer = jnp.exp(second_level - level)
    state = older[:, None, None] * first_state + newer[:, None, None] * second_state
    normal = older[:, None] * first_normal + newer[:, None] * second_normal
    return (state, normal, level, first_total + second_total)


def on_device_by_position(
    tokens,
    conv_value_weight,
    conv_gate_weight,
    conv_kernel,
    conv_norm_gain,
    query_weight,
    key_weight,
    value_weight,
    input_gate_weight,
    forget_gate_weight,
    input_offset,
    forget_offset,
    memory_norm_gain,
    conv_out_weight,
    memory_out_weight,
):
    length = tokens.shape[0]
    heads_here = input_gate_weight.shape[1]
    whole = lax.all_gather(tokens, "tp", axis=1, tiled=True)
    pieces = (
        lax.all_gather(conv_value_weight, "sp", axis=0, tiled=True),
        lax.all_gather(conv_gate_weight, "sp", axis=0, tiled=True),
        lax.all_gather(query_weight, "sp", axis=0, tiled=True),
        lax.all_gather(key_weight, "sp", axis=0, tiled=True),
        lax.all_gather(value_weight, "sp", axis=0, tiled=True),
    )
    folded = tuple((jnp.dot(whole, piece, preferred_element_type=jnp.float32) for piece in pieces))
    conv_value, conv_gate, query_flat, key_flat, value_flat = folded
    gate_pre = jnp.dot(whole, input_gate_weight, preferred_element_type=jnp.float32)
    forget_pre = jnp.dot(whole, forget_gate_weight, preferred_element_type=jnp.float32)
    glu = (conv_value * jax.nn.sigmoid(conv_gate)).astype(jnp.bfloat16)
    taps = conv_kernel.shape[0]
    head_dim = query_flat.shape[1] // heads_here

    def to_heads(flat):
        return flat.astype(jnp.bfloat16).reshape(length, heads_here, head_dim).transpose(1, 0, 2)

    query = to_heads(query_flat)
    key = to_heads(key_flat)
    value = to_heads(value_flat)
    gate_in = (gate_pre + input_offset).T
    forget_log = jax.nn.log_sigmoid(forget_pre + forget_offset).T
    within = jnp.cumsum(forget_log, axis=1)
    total = within[:, -1]
    end_log = total[:, None] - within + gate_in
    local_level = jnp.max(end_log, axis=1)
    fresh = jnp.exp(end_log - local_level[:, None])
    scaled_key = (fresh[:, :, None] * key).astype(jnp.bfloat16)
    local_state = jnp.einsum("hse,hsd->hed", value, scaled_key, preferred_element_type=jnp.float32)
    local_normal = jnp.sum(scaled_key.astype(jnp.float32), axis=1)
    blank_state = (
        jnp.zeros_like(local_state),
        jnp.zeros_like(local_normal),
        jnp.full_like(local_level, LOWEST_LEVEL),
        jnp.zeros_like(total),
    )
    prior = shifted_2(glu[length - (taps - 1) :], "sp", 1)
    incoming = carried_in(
        (local_state, local_normal, local_level, total), "sp", merge_states, blank_state
    )
    extended = jnp.concatenate([prior, glu], axis=0).astype(jnp.float32)
    conv = depthwise(extended, conv_kernel.astype(jnp.float32))
    blocks = length // BLOCK

    def split(array):
        return jnp.moveaxis(array.reshape((heads_here, blocks, BLOCK) + array.shape[2:]), 1, 0)

    _, hidden = lax.scan(
        block_step,
        tuple(incoming[:3]),
        (split(query), split(key), split(value), split(gate_in), split(forget_log)),
    )
    hidden = jnp.moveaxis(hidden, 0, 1).reshape(heads_here, length, head_dim)
    hidden_squares = jnp.sum(hidden * hidden, axis=(0, 2))
    channel_sum, channel_squares, memory_squares = lax.psum(
        (jnp.sum(conv, axis=1), jnp.sum(conv * conv, axis=1), hidden_squares), "tp"
    )
    channels = conv.shape[1] * lax.axis_size("tp")
    mean = (channel_sum / channels)[:, None]
    variance = (channel_squares / channels)[:, None] - mean * mean
    conv_branch = jax.nn.silu((conv - mean) * lax.rsqrt(variance + EPS) * conv_norm_gain).astype(
        jnp.bfloat16
    )
    entries = heads_here * head_dim * lax.axis_size("tp")
    memory_scale = lax.rsqrt(memory_squares / entries + EPS)
    hidden = hidden * memory_scale[None, :, None]
    hidden = hidden * memory_norm_gain.reshape(heads_here, 1, head_dim)
    memory_branch = (
        hidden.transpose(1, 0, 2).reshape(length, heads_here * head_dim).astype(jnp.bfloat16)
    )
    conv_columns, memory_columns = (
        lax.all_gather(conv_out_weight, "sp", axis=1, tiled=True),
        lax.all_gather(memory_out_weight, "sp", axis=1, tiled=True),
    )
    contract = (((0,), (1,)), ((), ()))
    summed = lax.psum_scatter(
        (
            lax.dot_general(conv_columns, conv_branch, contract, preferred_element_type=jnp.float32)
            + lax.dot_general(
                memory_columns, memory_branch, contract, preferred_element_type=jnp.float32
            )
        ).astype(jnp.bfloat16),
        "tp",
        scatter_dimension=0,
        tiled=True,
    ).astype(jnp.float32)
    return summed.T.astype(jnp.bfloat16)


def forget_parts(forget_log):
    coarse = jnp.round(forget_log * 8.0) * 0.125
    return (jnp.cumsum(coarse, axis=-1), jnp.cumsum(forget_log - coarse, axis=-1))


def exchange_weights(pieces):
    return lax.all_to_all(pieces, "sp", 0, 0, tiled=False)


def gather_tokens(tokens):
    whole = lax.all_gather(tokens, "tp", axis=1, tiled=True)
    return lax.all_gather(whole, "sp", axis=0, tiled=True)


def gather_in_group(mine, size):
    count = lax.axis_size("sp")
    groups = [list(range(first, first + size)) for first in range(0, count, size)]
    return lax.all_gather(mine, "sp", axis_index_groups=groups)


def on_device_by_column(
    tokens,
    conv_value_weight,
    conv_gate_weight,
    conv_kernel,
    conv_norm_gain,
    query_weight,
    key_weight,
    value_weight,
    input_gate_weight,
    forget_gate_weight,
    input_offset,
    forget_offset,
    memory_norm_gain,
    conv_out_weight,
    memory_out_weight,
):
    f32, bf16 = (jnp.float32, jnp.bfloat16)
    count = lax.axis_size("sp")
    columns = lax.axis_size("tp")
    place = lax.axis_index("sp")
    heads_here = input_gate_weight.shape[1]
    size = count // heads_here
    head, quarter = (place // size, place % size)
    depth = query_weight.shape[0]
    head_dim = query_weight.shape[1] // heads_here
    slab = head_dim // size
    channels = conv_value_weight.shape[1] // count
    pieces = jnp.concatenate(
        [
            w.reshape(depth, count, -1)
            for w in (query_weight, key_weight, value_weight, conv_value_weight, conv_gate_weight)
        ],
        axis=2,
    ).transpose(1, 0, 2)
    weights = exchange_weights(pieces).reshape(count * depth, -1)
    whole = gather_tokens(tokens)
    length = whole.shape[0]
    offsets = lax.all_gather(
        jnp.concatenate([input_offset, forget_offset], axis=1), "sp", axis=0, tiled=True
    )
    gate_weights = jnp.concatenate([input_gate_weight, forget_gate_weight], axis=1)
    flat = jnp.dot(whole, weights, preferred_element_type=f32)
    gates = (jnp.dot(whole, gate_weights, preferred_element_type=f32) + offsets).T
    glu = (
        flat[:, 3 * slab : 3 * slab + channels] * jax.nn.sigmoid(flat[:, 3 * slab + channels :])
    ).astype(bf16)
    parts = gather_in_group(flat[:, : 3 * slab].astype(bf16), size)
    taps = conv_kernel.shape[0]
    kernel = lax.dynamic_slice_in_dim(conv_kernel, place * channels, channels, 1).astype(f32)
    extended = jnp.concatenate([jnp.zeros((taps - 1, channels), f32), glu.astype(f32)], axis=0)
    conv = depthwise(extended, kernel)
    rows = length // size
    start = quarter * rows
    gate_in = lax.dynamic_index_in_dim(gates[:heads_here], head, 0, False)
    forget_log = jax.nn.log_sigmoid(lax.dynamic_index_in_dim(gates[heads_here:], head, 0, False))
    coarse, fine = forget_parts(forget_log)
    mine_coarse = lax.dynamic_slice_in_dim(coarse, start, rows)
    mine_fine = lax.dynamic_slice_in_dim(fine, start, rows)
    log_weight = (
        mine_coarse[:, None]
        - coarse[None, :]
        + (mine_fine[:, None] - fine[None, :])
        + gate_in[None, :]
    )
    causal = (start + jnp.arange(rows))[:, None] >= jnp.arange(length)[None, :]
    log_weight = jnp.where(causal, log_weight, -jnp.inf)
    weight = jnp.exp(log_weight - jnp.max(log_weight, axis=1, keepdims=True))
    query = lax.dynamic_slice_in_dim(parts[:, :, :slab], start, rows, 1)
    query = query.transpose(1, 0, 2).reshape(rows, head_dim)
    key = parts[:, :, slab : 2 * slab].transpose(1, 0, 2).reshape(length, head_dim)
    value = parts[:, :, 2 * slab :].transpose(1, 0, 2).reshape(length, head_dim)
    scores = jnp.einsum("td,sd->ts", query, key, preferred_element_type=f32) * (
        weight * head_dim ** (-0.5)
    )
    numer = jnp.dot(scores.astype(bf16), value, preferred_element_type=f32)
    denom = jnp.sum(scores, axis=1)
    cell = numer / jnp.maximum(jnp.abs(denom), 1.0)[:, None]
    squares = lax.dynamic_update_slice_in_dim(
        jnp.zeros((length,), f32), jnp.sum(cell * cell, axis=1), start, 0
    )
    sums = lax.psum(
        jnp.stack([jnp.sum(conv, axis=1), jnp.sum(conv * conv, axis=1), squares]), ("sp", "tp")
    )
    total = channels * count * columns
    mean = sums[0] / total
    variance = sums[1] / total - mean * mean
    gain = lax.dynamic_slice_in_dim(conv_norm_gain, place * channels, channels)
    conv_branch = jax.nn.silu(
        (conv - mean[:, None]) * lax.rsqrt(variance + EPS)[:, None] * gain
    ).astype(bf16)
    entries = heads_here * head_dim * columns
    memory_scale = lax.rsqrt(lax.dynamic_slice_in_dim(sums[2], start, rows) / entries + EPS)
    memory_gain = lax.dynamic_slice_in_dim(memory_norm_gain, head * head_dim, head_dim)
    memory_branch = (cell * memory_scale[:, None] * memory_gain).astype(bf16)
    conv_all = lax.all_gather(conv_branch, "sp")
    memory_all = lax.all_gather(memory_branch, "sp")
    conv_all = conv_all.transpose(1, 0, 2).reshape(length, -1)
    memory_all = (
        memory_all.reshape(heads_here, length, head_dim).transpose(1, 0, 2).reshape(length, -1)
    )
    partial = (
        jnp.dot(conv_all, conv_out_weight, preferred_element_type=f32)
        + jnp.dot(memory_all, memory_out_weight, preferred_element_type=f32)
    ).astype(bf16)
    return send_partials(partial)


def send_partials(partial):
    count, columns = (lax.axis_size("sp"), lax.axis_size("tp"))
    length, width = partial.shape
    swapped = lax.all_to_all(partial.reshape(count, length // count, width), "sp", 0, 0)
    swapped = swapped.reshape(columns, count // columns, length // count, width)
    groups = lax.all_to_all(swapped, "tp", 0, 0)
    summed = jnp.sum(groups.astype(jnp.float32), axis=0).astype(jnp.bfloat16)
    return summed.transpose(1, 0, 2).reshape(length // count, -1)


def splits_by_column(mesh, tokens, query_weight, conv_value_weight, input_gate_weight):
    count, columns = (mesh.shape["sp"], mesh.shape["tp"])
    heads_here = input_gate_weight.shape[1] // columns
    head_dim = query_weight.shape[1] // input_gate_weight.shape[1]
    if count % heads_here or count % columns:
        return False
    size = count // heads_here
    return (
        tokens.size * 2 <= 8 * 2**20
        and head_dim % size == 0
        and (tokens.shape[0] % (size * 8) == 0)
        and (conv_value_weight.shape[1] % (count * columns) == 0)
    )


def solution(mesh):
    in_specs = (
        P("sp", "tp"),
        P("sp", "tp"),
        P("sp", "tp"),
        P(None, "tp"),
        P("tp"),
        P("sp", "tp"),
        P("sp", "tp"),
        P("sp", "tp"),
        P(None, "tp"),
        P(None, "tp"),
        P("sp", "tp"),
        P("sp", "tp"),
        P("tp"),
        P("tp", "sp"),
        P("tp", "sp"),
    )
    out_specs = P("sp", "tp")

    def run(*arrays):
        by_column = splits_by_column(mesh, arrays[0], arrays[5], arrays[1], arrays[8])
        on_device = on_device_by_column if by_column else on_device_by_position
        return jax.shard_map(
            on_device, mesh=mesh, in_specs=in_specs, out_specs=out_specs, check_vma=False
        )(*arrays)

    return run
```

profile of v0, /device:TPU:0, one launch (start us, length us, event | category | flops | bytes accessed | tf_op | source)
XLA Modules:
  0.0 270.2 jit_solution(7886336359932702150)
XLA Ops:
  6.6 10.4 %all_gather.27 = bf16[128,2048]{1,0:T(8,128)(2,1)} all-gather(bf16[128,512]{1,0:T(8,128)(2,1)} %param.15), channel_id=1, replica_groups=mesh['sp'=8,'tp'=4] {'tp'}, dimensions={1}, use_global_device_ids=true | all-gather | bytes 655360 | tf_op jit(solution)/shard_map/all_gather | solution.py:219
  17.0 1.1 copy.40
  18.1 1.1 copy.41
  19.2 1.1 copy.42
  20.3 1.0 copy.43
  21.3 1.0 copy.44
  22.3 0.7 constant_dynamic-update-slice_fusion.4
  23.0 0.7 constant_dynamic-update-slice_fusion.3
  23.7 0.7 constant_dynamic-update-slice_fusion.2
  24.4 0.7 constant_dynamic-update-slice_fusion.1
  25.1 0.7 constant_dynamic-update-slice_fusion
  25.8 5.8 %all-to-all-start = ((bf16[8,256,256]{1,2,0:T(8,128)(2,1)}), bf16[8,256,256]{1,2,0:T(8,128)(2,1)S(1)}, u32[]{:S(2)}, u32[]{:S(2)}) async-start(bf16[8,256,256]{1,2,0:T(8,128)(2,1)} %bitcast.5), calls=%async_computation | async-start | bytes 2097152 | tf_op jit(solution)/shard_map/all_to_all | solution.py:215
  31.7 0.1 dynamic-slice_convert_fusion
  31.8 37.1 %all-to-all-done = bf16[8,256,256]{1,2,0:T(8,128)(2,1)S(1)} async-done(((bf16[8,256,256]{1,2,0:T(8,128)(2,1)}), bf16[8,256,256]{1,2,0:T(8,128)(2,1)S(1)}, u32[]{:S(2)}, u32[]{:S(2)}) %all-to-all-start) | async-done | bytes 1048608 | tf_op jit(solution)/shard_map/all_to_all | solution.py:215
  68.9 0.5 copy.45
  69.4 37.1 %all-gather.7.cloned.1.call-done = bf16[1024,2048]{1,0:T(8,128)(2,1)} async-done(((bf16[128,2048]{1,0:T(8,128)(2,1)}), bf16[1024,2048]{1,0:T(8,128)(2,1)}) %all-gather.7.cloned.1.call-update) | async-done | bytes 4194320 | tf_op jit(solution)/shard_map/all_gather | solution.py:220
  106.5 3.5 %convolution_bitcast_fusion.1 = f32[1024,256]{0,1:T(8,128)S(1)} fusion(bf16[2048,256]{1,0:T(8,128)(2,1)S(1)} %bitcast.143, bf16[1024,2048]{1,0:T(8,128)(2,1)} %all-gather.7.cloned.1.call-done), kind=kOutput, calls=%fused_computation.3 | convolution fusion | flops 1073741824 | bytes 6291456 | tf_op jit(solution)/shard_map/dot_general | solution.py:271
  110.0 0.8 slice.659
  110.9 0.1 dynamic_slice.36
  111.0 27.4 %all_gather.31 = f32[1024,4]{0,1:T(4,128)S(1)} all-gather(f32[128,4]{0,1:T(4,128)S(1)} %pad_maximum_fusion.1), channel_id=1, replica_groups=mesh['sp'=8,'tp'=4] {'sp'}, dimensions={0}, use_global_device_ids=true | all-gather | bytes 18432 | tf_op jit(solution)/shard_map/all_gather | solution.py:267
  138.5 3.4 %fusion.3 = f32[4,1024]{1,0:T(4,128)S(1)} fusion(f32[1024,4]{0,1:T(4,128)S(1)} %all_gather.31, bf16[1024,2048]{1,0:T(8,128)(2,1)} %all-gather.7.cloned.1.call-done, bf16[2048,2]{0,1:T(2,128)(2,1)S(1)} %copy-done.2, bf16[2048,2]{0,1:T(2,128)(2,1)S(1)} %copy-done.3), kind=kOutput, calls=%fused_computation.8 | convolution fusion | flops 16814080 | bytes 4243456 | tf_op jit(solution)/shard_map/dot_general | solution.py:272
  141.9 0.3 reduce-window.24
  142.2 0.1 slice.300
  142.3 0.3 reduce-window.16
  142.7 0.1 slice_reduce_fusion
  142.8 0.1 slice_reduce_fusion.1
  143.1 0.5 fusion.4
  143.6 1.3 fusion.81
  144.9 0.4 all-gather.9.cloned.1.call-done
  145.3 2.9 %reshape.162 = bf16[4,1024,192]{1,0,2:T(4,128)(2,1)S(1)} reshape(bf16[4096,192]{0,1:T(8,128)(2,1)} %all-gather.9.cloned.1.call-done) | data formatting | bytes 3145728 | tf_op jit(solution)/shard_map/all_gather | solution.py:226
  148.2 0.5 fusion.83
  148.8 0.7 fusion.85
  149.5 0.2 copy.56
  149.7 0.4 multiply_reduce_fusion
  150.1 39.6 %psum.7 = f32[3,1024]{1,0:T(4,128)S(1)} all-reduce(f32[3,1024]{1,0:T(4,128)S(1)} %pad_maximum_fusion), channel_id=1, replica_groups=mesh['sp'=8,'tp'=4] {'sp','tp'}, use_global_device_ids=true, to_apply=%region_9.10 | all-reduce | flops 3072 | bytes 24576 | tf_op jit(solution)/shard_map/psum | solution.py:310
  189.8 0.8 multiply_convert_fusion
  190.6 0.1 dynamic_slice.34
  190.6 0.1 multiply_convert_fusion.1
  190.8 31.8 %all-gather.1 = bf16[8192,32]{0,1:T(8,128)(2,1)S(1)} all-gather(bf16[1024,32]{0,1:T(8,128)(2,1)S(1)} %multiply_convert_fusion.1), channel_id=3, replica_groups=mesh['sp'=8,'tp'=4] {'sp'}, dimensions={0}, use_global_device_ids=true | all-gather | bytes 589824 | tf_op jit(solution)/shard_map/all_gather | solution.py:324
  222.6 9.4 %all-gather.11.cloned.1.call-done = bf16[2048,256]{0,1:T(8,128)(2,1)} async-done(((bf16[256,256]{0,1:T(8,128)(2,1)}), bf16[2048,256]{0,1:T(8,128)(2,1)}) %all-gather.11.cloned.1.call-update) | async-done | bytes 1048592 | tf_op jit(solution)/shard_map/all_gather | solution.py:325
  232.0 1.3 copy.69
  233.3 0.5 fusion.86
  233.8 0.4 fusion.1
  234.2 17.2 %all_to_all.15 = bf16[8,128,256]{2,1,0:T(8,128)(2,1)S(1)} all-to-all(bf16[8,128,256]{2,1,0:T(8,128)(2,1)S(1)} %bitcast.139), channel_id=1, replica_groups=mesh['sp'=8,'tp'=4] {'sp'}, dimensions={0} | all-to-all | bytes 1048576 | tf_op jit(solution)/shard_map/all_to_all | solution.py:340
  251.3 11.3 %all_to_all.16 = bf16[4,2,128,256]{3,2,1,0:T(8,128)(2,1)S(1)} all-to-all(bf16[4,2,128,256]{3,2,1,0:T(8,128)(2,1)S(1)} %bitcast.141), channel_id=1, replica_groups=mesh['sp'=8,'tp'=4] {'tp'}, dimensions={0} | all-to-all | bytes 1048576 | tf_op jit(solution)/shard_map/all_to_all | solution.py:342
  262.7 0.1 reduce_sum.52
  262.8 0.1 copy.51
  262.9 0.8 copy.52
  (48 shorter events, 0.8 us)
Async XLA Ops:
  6.5 226.8 %copy-start = (bf16[512,256]{1,0:T(8,128)(2,1)S(1)}, bf16[512,256]{1,0:T(8,128)(2,1)}, u32[]{:S(2)}) copy-start(bf16[512,256]{1,0:T(8,128)(2,1)} %param.29) | copy-start | bytes 786436
  6.5 25.1 %copy-start.5 = (f32[128,2]{0,1:T(2,128)S(1)}, f32[128,2]{0,1:T(2,128)}, u32[]{:S(2)}) copy-start(f32[128,2]{0,1:T(2,128)} %param.26) | copy-start | bytes 3076
  6.5 25.1 %copy-start.6 = (f32[128,2]{0,1:T(2,128)S(1)}, f32[128,2]{0,1:T(2,128)}, u32[]{:S(2)}) copy-start(f32[128,2]{0,1:T(2,128)} %param.25) | copy-start | bytes 3076
  6.5 25.1 %copy-start.4 = (bf16[31,256]{1,0:T(8,128)(2,1)S(1)}, bf16[31,256]{1,0:T(8,128)(2,1)}, u32[]{:S(2)}) copy-start(bf16[31,256]{1,0:T(8,128)(2,1)} %param.18) | copy-start | bytes 47620
  6.5 99.9 %all-gather.7.cloned.1.call-start = ((), (), s32[]{:S(2)}) async-start(), calls=%async_computation.3 | async-start | bytes 4718592 | tf_op jit(solution)/shard_map/all_gather | solution.py:220
  25.8 43.1 %all-to-all-start = ((bf16[8,256,256]{1,2,0:T(8,128)(2,1)}), bf16[8,256,256]{1,2,0:T(8,128)(2,1)S(1)}, u32[]{:S(2)}, u32[]{:S(2)}) async-start(bf16[8,256,256]{1,2,0:T(8,128)(2,1)} %bitcast.5), calls=%async_computation | async-start | bytes 2097152 | tf_op jit(solution)/shard_map/all_to_all | solution.py:215
  31.6 113.7 %all-gather.9.cloned.1.call-start = ((), (), s32[]{:S(2)}) async-start(), calls=%async_computation.4 | async-start | bytes 1966080 | tf_op jit(solution)/shard_map/all_gather | solution.py:226
  106.5 4.5 %copy-start.7 = (f32[512]{0:T(512)S(1)}, f32[512]{0:T(512)}, u32[]{:S(2)}) copy-start(f32[512]{0:T(512)} %param.27) | copy-start | bytes 6148
  106.5 32.0 %copy-start.2 = (bf16[2048,2]{0,1:T(2,128)(2,1)S(1)}, bf16[2048,2]{0,1:T(2,128)(2,1)}, u32[]{:S(2)}) copy-start(bf16[2048,2]{0,1:T(2,128)(2,1)} %param.24) | copy-start | bytes 24580
  106.5 32.0 %copy-start.3 = (bf16[2048,2]{0,1:T(2,128)(2,1)S(1)}, bf16[2048,2]{0,1:T(2,128)(2,1)}, u32[]{:S(2)}) copy-start(bf16[2048,2]{0,1:T(2,128)(2,1)} %param.23) | copy-start | bytes 24580
  110.8 121.2 %all-gather.11.cloned.1.call-start = ((), (), s32[]{:S(2)}) async-start(), calls=%async_computation.5 | async-start | bytes 1179648 | tf_op jit(solution)/shard_map/all_gather | solution.py:325
  148.8 41.8 %copy-start.8 = (f32[256]{0:T(256)S(1)}, f32[256]{0:T(256)}, u32[]{:S(2)}) copy-start(f32[256]{0:T(256)} %param.19) | copy-start | bytes 3076
  149.7 84.1 %copy-start.1 = (bf16[256,256]{1,0:T(8,128)(2,1)S(1)}, bf16[256,256]{1,0:T(8,128)(2,1)}, u32[]{:S(2)}) copy-start(bf16[256,256]{1,0:T(8,128)(2,1)} %param.28) | copy-start | bytes 393220
Sparse Core Ops, SparseCore 0:
  17.1 89.3 all-gather.6
  110.9 34.2 all-gather.8
  190.7 41.2 all-gather.10
where the time goes:
time: 271 us; the launch traced here: 270 us
  blocking collectives  138 us (51%)
  waiting for transfers between devices  83.9 us (31%)
  local copies, waits for them, and re-layouts  16.7 us (6%)
  between operations  13.5 us (5%)
  matrix products  8.81 us (3%)
  starting transfers between devices  5.92 us (2%)
  other arithmetic  3.6 us (1%)
    psum x1, blocking collectives, on_device_by_column(): lax.psum(jnp.stack([jnp.sum(conv, axis=1), jnp.sum(conv * conv, axis=1),...  39.6 us
    all_to_all x1, waiting for transfers between devices, exchange_weights(): return lax.all_to_all(pieces, 'sp', 0, 0, tiled=False)  37.1 us
    all_gather x1, waiting for transfers between devices, gather_tokens(): return lax.all_gather(whole, 'sp', axis=0, tiled=True)  37.1 us
    all_gather x1, blocking collectives, on_device_by_column(): conv_all = lax.all_gather(conv_branch, 'sp')  31.8 us
    all_gather x1, blocking collectives, on_device_by_column(): lax.all_gather(jnp.concatenate([input_offset, forget_offset], axis=1), 's...  27.4 us
    all_to_all x1, blocking collectives, send_partials(): lax.all_to_all(partial.reshape(count, length // count, width), 'sp', 0, 0)  17.2 us
    all_to_all x1, blocking collectives, send_partials(): groups = lax.all_to_all(swapped, 'tp', 0, 0)  11.3 us
    all_gather x1, blocking collectives, gather_tokens(): whole = lax.all_gather(tokens, 'tp', axis=1, tiled=True)  10.4 us
  transfers between devices with their start and end apart: 4, of which 4 were waited for; matrix products, arithmetic and copies ran while one was open for 6% of the time, Pallas kernels for 0%

commit v1 on v0

--- a/solution.py
+++ b/solution.py
@@ -307,8 +307,11 @@
     squares = lax.dynamic_update_slice_in_dim(
         jnp.zeros((length,), f32), jnp.sum(cell * cell, axis=1), start, 0
     )
-    sums = lax.psum(
-        jnp.stack([jnp.sum(conv, axis=1), jnp.sum(conv * conv, axis=1), squares]), ("sp", "tp")
+    sums = jnp.sum(
+        lax.all_gather(
+            jnp.stack([jnp.sum(conv, axis=1), jnp.sum(conv * conv, axis=1), squares]), ("sp", "tp")
+        ),
+        axis=0,
     )
     total = channels * count * columns
     mean = sums[0] / total

time: 271 us -> 269 us (level)
  waiting for transfers between devices: 83.9 us -> 79.3 us
    all_gather x0 -> x1, blocking collectives: none -> 41.8 us  [on_device_by_column(): lax.all_gather(jnp.stack([jnp.sum(conv, axis=1), jnp.sum(conv * conv, axi...]
    psum x1 -> x0, blocking collectives: 39.6 us -> none  [on_device_by_column(): lax.psum(jnp.stack([jnp.sum(conv, axis=1), jnp.sum(conv * conv, axis=1),...]
    all_gather x1, waiting for transfers between devices: 9.39 us -> 4.7 us  [on_device_by_column(): memory_all = lax.all_gather(memory_branch, 'sp')]
where the time goes in v1:
time: 269 us; the launch traced here: 268 us
  blocking collectives  140 us (52%)
  waiting for transfers between devices  79.3 us (29%)
  local copies, waits for them, and re-layouts  16.7 us (6%)
  between operations  13.5 us (5%)
  matrix products  8.82 us (3%)
  starting transfers between devices  5.92 us (2%)
  other arithmetic  3.7 us (1%)
    all_gather x1, blocking collectives, on_device_by_column(): lax.all_gather(jnp.stack([jnp.sum(conv, axis=1), jnp.sum(conv * conv, axi...  41.8 us
    all_to_all x1, waiting for transfers between devices, exchange_weights(): return lax.all_to_all(pieces, 'sp', 0, 0, tiled=False)  37.1 us
    all_gather x1, waiting for transfers between devices, gather_tokens(): return lax.all_gather(whole, 'sp', axis=0, tiled=True)  37.1 us
    all_gather x1, blocking collectives, on_device_by_column(): conv_all = lax.all_gather(conv_branch, 'sp')  32.3 us
    all_gather x1, blocking collectives, on_device_by_column(): lax.all_gather(jnp.concatenate([input_offset, forget_offset], axis=1), 's...  27.4 us
    all_to_all x1, blocking collectives, send_partials(): lax.all_to_all(partial.reshape(count, length // count, width), 'sp', 0, 0)  17.2 us
    all_to_all x1, blocking collectives, send_partials(): groups = lax.all_to_all(swapped, 'tp', 0, 0)  11.2 us
    all_gather x1, blocking collectives, gather_tokens(): whole = lax.all_gather(tokens, 'tp', axis=1, tiled=True)  10.4 us
  transfers between devices with their start and end apart: 4, of which 4 were waited for; matrix products, arithmetic and copies ran while one was open for 6% of the time, Pallas kernels for 0%

profile of v1, /device:TPU:0, one launch (start us, length us, event | category | flops | bytes accessed | tf_op | source)
XLA Modules:
  0.0 268.2 jit_solution(7176021752319690707)
XLA Ops:
  6.6 10.4 %all_gather.33 = bf16[128,2048]{1,0:T(8,128)(2,1)} all-gather(bf16[128,512]{1,0:T(8,128)(2,1)} %param.15), channel_id=1, replica_groups=mesh['sp'=8,'tp'=4] {'tp'}, dimensions={1}, use_global_device_ids=true | all-gather | bytes 655360 | tf_op jit(solution)/shard_map/all_gather | solution.py:219
  17.0 1.1 copy.40
  18.1 1.1 copy.41
  19.2 1.1 copy.42
  20.3 1.0 copy.43
  21.3 1.0 copy.44
  22.3 0.7 constant_dynamic-update-slice_fusion.4
  23.0 0.7 constant_dynamic-update-slice_fusion.3
  23.7 0.7 constant_dynamic-update-slice_fusion.2
  24.4 0.7 constant_dynamic-update-slice_fusion.1
  25.1 0.7 constant_dynamic-update-slice_fusion
  25.8 5.8 %all-to-all-start = ((bf16[8,256,256]{1,2,0:T(8,128)(2,1)}), bf16[8,256,256]{1,2,0:T(8,128)(2,1)S(1)}, u32[]{:S(2)}, u32[]{:S(2)}) async-start(bf16[8,256,256]{1,2,0:T(8,128)(2,1)} %bitcast.5), calls=%async_computation | async-start | bytes 2097152 | tf_op jit(solution)/shard_map/all_to_all | solution.py:215
  31.7 0.1 dynamic-slice_convert_fusion
  31.8 37.1 %all-to-all-done = bf16[8,256,256]{1,2,0:T(8,128)(2,1)S(1)} async-done(((bf16[8,256,256]{1,2,0:T(8,128)(2,1)}), bf16[8,256,256]{1,2,0:T(8,128)(2,1)S(1)}, u32[]{:S(2)}, u32[]{:S(2)}) %all-to-all-start) | async-done | bytes 1048608 | tf_op jit(solution)/shard_map/all_to_all | solution.py:215
  68.9 0.5 copy.45
  69.4 37.1 %all-gather.9.cloned.1.call-done = bf16[1024,2048]{1,0:T(8,128)(2,1)} async-done(((bf16[128,2048]{1,0:T(8,128)(2,1)}), bf16[1024,2048]{1,0:T(8,128)(2,1)}) %all-gather.9.cloned.1.call-update) | async-done | bytes 4194320 | tf_op jit(solution)/shard_map/all_gather | solution.py:220
  106.5 3.5 %convolution_bitcast_fusion.1 = f32[1024,256]{0,1:T(8,128)S(1)} fusion(bf16[2048,256]{1,0:T(8,128)(2,1)S(1)} %bitcast.145, bf16[1024,2048]{1,0:T(8,128)(2,1)} %all-gather.9.cloned.1.call-done), kind=kOutput, calls=%fused_computation.3 | convolution fusion | flops 1073741824 | bytes 6291456 | tf_op jit(solution)/shard_map/dot_general | solution.py:271
  110.0 0.8 slice.659
  110.9 0.1 dynamic_slice.36
  111.0 27.4 %all_gather.37 = f32[1024,4]{0,1:T(4,128)S(1)} all-gather(f32[128,4]{0,1:T(4,128)S(1)} %pad_maximum_fusion), channel_id=1, replica_groups=mesh['sp'=8,'tp'=4] {'sp'}, dimensions={0}, use_global_device_ids=true | all-gather | bytes 18432 | tf_op jit(solution)/shard_map/all_gather | solution.py:267
  138.5 3.4 %fusion.3 = f32[4,1024]{1,0:T(4,128)S(1)} fusion(f32[1024,4]{0,1:T(4,128)S(1)} %all_gather.37, bf16[1024,2048]{1,0:T(8,128)(2,1)} %all-gather.9.cloned.1.call-done, bf16[2048,2]{0,1:T(2,128)(2,1)S(1)} %copy-done.2, bf16[2048,2]{0,1:T(2,128)(2,1)S(1)} %copy-done.3), kind=kOutput, calls=%fused_computation.8 | convolution fusion | flops 16814080 | bytes 4243456 | tf_op jit(solution)/shard_map/dot_general | solution.py:272
  141.9 0.3 reduce-window.24
  142.3 0.3 reduce-window.16
  142.7 0.1 slice_reduce_fusion
  142.8 0.1 slice_reduce_fusion.1
  143.1 0.5 fusion.4
  143.6 1.3 fusion.81
  144.9 0.4 all-gather.11.cloned.1.call-done
  145.3 2.9 %reshape.162 = bf16[4,1024,192]{1,0,2:T(4,128)(2,1)S(1)} reshape(bf16[4096,192]{0,1:T(8,128)(2,1)} %all-gather.11.cloned.1.call-done) | data formatting | bytes 3145728 | tf_op jit(solution)/shard_map/all_gather | solution.py:226
  148.2 0.5 fusion.83
  148.8 0.7 fusion.85
  149.5 0.2 copy.56
  149.7 0.4 multiply_reduce_fusion
  150.1 41.8 %all-gather.4 = f32[32,3,1024]{2,1,0:T(4,128)S(1)} all-gather(f32[1,3,1024]{2,1,0:T(4,128)S(1)} %maximum_bitcast_fusion), channel_id=3, replica_groups=mesh['sp'=8,'tp'=4] {'sp','tp'}, dimensions={0}, use_global_device_ids=true | all-gather | bytes 405504 | tf_op jit(solution)/shard_map/all_gather | solution.py:311
  191.9 0.1 reduce_sum.61
  192.1 0.8 multiply_convert_fusion
  192.9 0.1 dynamic_slice.34
  193.0 0.1 multiply_convert_fusion.1
  193.1 32.3 %all-gather.2 = bf16[8192,32]{0,1:T(8,128)(2,1)S(1)} all-gather(bf16[1024,32]{0,1:T(8,128)(2,1)S(1)} %multiply_convert_fusion.1), channel_id=4, replica_groups=mesh['sp'=8,'tp'=4] {'sp'}, dimensions={0}, use_global_device_ids=true | all-gather | bytes 589824 | tf_op jit(solution)/shard_map/all_gather | solution.py:327
  225.4 4.7 %all-gather.13.cloned.1.call-done = bf16[2048,256]{0,1:T(8,128)(2,1)} async-done(((bf16[256,256]{0,1:T(8,128)(2,1)}), bf16[2048,256]{0,1:T(8,128)(2,1)}) %all-gather.13.cloned.1.call-update) | async-done | bytes 1048592 | tf_op jit(solution)/shard_map/all_gather | solution.py:328
  230.1 1.3 copy.69
  231.4 0.5 fusion.86
  231.9 0.4 fusion.1
  232.3 17.2 %all_to_all.15 = bf16[8,128,256]{2,1,0:T(8,128)(2,1)S(1)} all-to-all(bf16[8,128,256]{2,1,0:T(8,128)(2,1)S(1)} %bitcast.141), channel_id=1, replica_groups=mesh['sp'=8,'tp'=4] {'sp'}, dimensions={0} | all-to-all | bytes 1048576 | tf_op jit(solution)/shard_map/all_to_all | solution.py:343
  249.5 11.2 %all_to_all.16 = bf16[4,2,128,256]{3,2,1,0:T(8,128)(2,1)S(1)} all-to-all(bf16[4,2,128,256]{3,2,1,0:T(8,128)(2,1)S(1)} %bitcast.143), channel_id=1, replica_groups=mesh['sp'=8,'tp'=4] {'tp'}, dimensions={0} | all-to-all | bytes 1048576 | tf_op jit(solution)/shard_map/all_to_all | solution.py:345
  260.7 0.1 reduce_sum.62
  260.8 0.1 copy.51
  260.9 0.8 copy.52
  (49 shorter events, 0.9 us)
Async XLA Ops:
  6.5 224.9 %copy-start = (bf16[512,256]{1,0:T(8,128)(2,1)S(1)}, bf16[512,256]{1,0:T(8,128)(2,1)}, u32[]{:S(2)}) copy-start(bf16[512,256]{1,0:T(8,128)(2,1)} %param.29) | copy-start | bytes 786436
  6.5 25.1 %copy-start.5 = (f32[128,2]{0,1:T(2,128)S(1)}, f32[128,2]{0,1:T(2,128)}, u32[]{:S(2)}) copy-start(f32[128,2]{0,1:T(2,128)} %param.26) | copy-start | bytes 3076
  6.5 25.1 %copy-start.6 = (f32[128,2]{0,1:T(2,128)S(1)}, f32[128,2]{0,1:T(2,128)}, u32[]{:S(2)}) copy-start(f32[128,2]{0,1:T(2,128)} %param.25) | copy-start | bytes 3076
  6.5 25.1 %copy-start.4 = (bf16[31,256]{1,0:T(8,128)(2,1)S(1)}, bf16[31,256]{1,0:T(8,128)(2,1)}, u32[]{:S(2)}) copy-start(bf16[31,256]{1,0:T(8,128)(2,1)} %param.18) | copy-start | bytes 47620
  6.5 99.9 %all-gather.9.cloned.1.call-start = ((), (), s32[]{:S(2)}) async-start(), calls=%async_computation.3 | async-start | bytes 4718592 | tf_op jit(solution)/shard_map/all_gather | solution.py:220
  25.8 43.1 %all-to-all-start = ((bf16[8,256,256]{1,2,0:T(8,128)(2,1)}), bf16[8,256,256]{1,2,0:T(8,128)(2,1)S(1)}, u32[]{:S(2)}, u32[]{:S(2)}) async-start(bf16[8,256,256]{1,2,0:T(8,128)(2,1)} %bitcast.5), calls=%async_computation | async-start | bytes 2097152 | tf_op jit(solution)/shard_map/all_to_all | solution.py:215
  31.6 113.7 %all-gather.11.cloned.1.call-start = ((), (), s32[]{:S(2)}) async-start(), calls=%async_computation.4 | async-start | bytes 1966080 | tf_op jit(solution)/shard_map/all_gather | solution.py:226
  106.5 4.5 %copy-start.7 = (f32[512]{0:T(512)S(1)}, f32[512]{0:T(512)}, u32[]{:S(2)}) copy-start(f32[512]{0:T(512)} %param.27) | copy-start | bytes 6148
  106.5 32.0 %copy-start.2 = (bf16[2048,2]{0,1:T(2,128)(2,1)S(1)}, bf16[2048,2]{0,1:T(2,128)(2,1)}, u32[]{:S(2)}) copy-start(bf16[2048,2]{0,1:T(2,128)(2,1)} %param.24) | copy-start | bytes 24580
  106.5 32.0 %copy-start.3 = (bf16[2048,2]{0,1:T(2,128)(2,1)S(1)}, bf16[2048,2]{0,1:T(2,128)(2,1)}, u32[]{:S(2)}) copy-start(bf16[2048,2]{0,1:T(2,128)(2,1)} %param.23) | copy-start | bytes 24580
  110.8 119.3 %all-gather.13.cloned.1.call-start = ((), (), s32[]{:S(2)}) async-start(), calls=%async_computation.5 | async-start | bytes 1179648 | tf_op jit(solution)/shard_map/all_gather | solution.py:328
  148.8 44.1 %copy-start.8 = (f32[256]{0:T(256)S(1)}, f32[256]{0:T(256)}, u32[]{:S(2)}) copy-start(f32[256]{0:T(256)} %param.19) | copy-start | bytes 3076
  150.1 81.8 %copy-start.1 = (bf16[256,256]{1,0:T(8,128)(2,1)S(1)}, bf16[256,256]{1,0:T(8,128)(2,1)}, u32[]{:S(2)}) copy-start(bf16[256,256]{1,0:T(8,128)(2,1)} %param.28) | copy-start | bytes 393220
Sparse Core Ops, SparseCore 0:
  17.1 89.3 all-gather.8
  110.9 34.2 all-gather.10
  193.0 37.0 all-gather.12
